TPU v7x, 32 devices: a whole 2x2x4 slice. The times are simulated.
32 devices in a mesh: ep: 8 (over z, core), tp: 4 (over y, x).
Axes of the slice: x: 2, y: 2, z: 4, core: 2. Of those that a mesh axis runs over, the one named last changes fastest.
Arguments:
- tokens: bfloat16 [384, 2048], P('ep'), may hold values from -6 to 6
- retention_state: float32 [384, 16, 64, 64], P('ep', 'tp'), may hold values from -1.5 to 1.5
- lengths: int32 [384], P('ep'), may hold values from 1024 to 16383
- query_weight: bfloat16 [2048, 1024], P(None, 'tp'), may hold values from -0.125 to 0.125
- key_weight: bfloat16 [2048, 1024], P(None, 'tp'), may hold values from -0.125 to 0.125
- value_weight: bfloat16 [2048, 1024], P(None, 'tp'), may hold values from -0.125 to 0.125
- gate_weight: bfloat16 [2048, 1024], P(None, 'tp'), may hold values from -0.125 to 0.125
- out_weight: bfloat16 [1024, 2048], P(None, 'tp'), may hold values from -0.1875 to 0.1875
- first_gain: float32 [2048], replicated, may hold values from 0.1 to 1.9
- routing: int32 [384, 4], P('ep'), may hold values from 0 to 31, all different within a row; in each aligned block of 48 rows (0 to 47, 48 to 95, ...) at most 18 rows name the same one
- route_weight: float32 [384, 4], P('ep'), may hold values from 0.1 to 1
- expert_gate: bfloat16 [32, 2048, 512], P('ep', None, 'tp'), may hold values from -0.125 to 0.125
- expert_up: bfloat16 [32, 2048, 512], P('ep', None, 'tp'), may hold values from -0.125 to 0.125
- expert_down: bfloat16 [32, 512, 2048], P('ep', None, 'tp'), may hold values from -0.25 to 0.25
- shared_gate: bfloat16 [2048, 512], P(None, 'tp'), may hold values from -0.125 to 0.125
- shared_up: bfloat16 [2048, 512], P(None, 'tp'), may hold values from -0.125 to 0.125
- shared_down: bfloat16 [512, 2048], P(None, 'tp'), may hold values from -0.25 to 0.25
- side_gate: bfloat16 [2048, 256], P('ep', 'tp'), may hold values from -0.125 to 0.125
- side_up: bfloat16 [2048, 256], P('ep', 'tp'), may hold values from -0.125 to 0.125
- side_down: bfloat16 [256, 2048], P(None, 'tp'), may hold values from -0.375 to 0.375
- side_switch: bfloat16 [2048], replicated, may hold values from -0.125 to 0.125
- second_gain: float32 [2048], P('tp'), may hold values from 0.1 to 1.9
Outputs:
- output: bfloat16 [384, 2048], P('ep', 'tp')
- new_state: float32 [384, 16, 64, 64], P('ep', 'tp')
Inputs may be any that keep to these rules, and one draw needn't show every extreme that they name: `routing`: each row names 4 different experts. Among the rows of one ep index (aligned blocks of 48 rows) no expert is named by more than 18 rows, a bound that some block reaches.
All inputs are finite; a program needn't handle non-finite values.
Results may differ from a plain program's by a relative error of at most 0.013.
Values may be sent and summed in bfloat16 or wider, within the bound.
A program may use at most 64 MiB of HBM per device.

v0:
```python
import jax
import jax.numpy as jnp
from jax import lax
from jax.sharding import PartitionSpec as P

HEADS = 16
RESIDUAL_SCALE = 2.0**0.25
NORM_EPS = 1e-05
GROUP_EPS = 1e-06
ROPE_BASE = 10000.0


def rotate(vector, positions):
    half_width = vector.shape[-1] // 2
    frequency = ROPE_BASE ** (-jnp.arange(half_width, dtype=jnp.float32) / half_width)
    angles = positions.astype(jnp.float32)[:, None, None] * frequency[None, None, :]
    cosine = jnp.cos(angles)
    sine_part = jnp.sin(angles)
    first_half = vector[..., :half_width]
    second_half = vector[..., half_width:]
    return jnp.concatenate(
        [
            first_half * cosine - second_half * sine_part,
            second_half * cosine + first_half * sine_part,
        ],
        -1,
    )


def retain(
    tokens,
    retention_state,
    lengths,
    query_weight,
    key_weight,
    value_weight,
    gate_weight,
    first_head,
):
    row_count = tokens.shape[0]
    head_count = retention_state.shape[1]
    head_width = retention_state.shape[2]

    def project(weight):
        rounded = jnp.dot(tokens, weight, preferred_element_type=jnp.float32).astype(jnp.bfloat16)
        return lax.optimization_barrier(rounded).astype(jnp.float32)

    queries = rotate(project(query_weight).reshape(row_count, head_count, head_width), lengths)
    key_rows = rotate(
        project(key_weight).reshape(row_count, head_count, head_width), lengths
    ) * head_width ** (-0.5)
    values = project(value_weight).reshape(row_count, head_count, head_width)
    gate_act = project(gate_weight)
    head_index = (first_head + jnp.arange(head_count)).astype(jnp.float32)
    decays = 1.0 - 2.0 ** (-5.0 - 7.0 * head_index / (HEADS - 1))
    own_term = jnp.sum(queries * key_rows, -1, keepdims=True) * values
    carried = decays[None, :, None] * jnp.einsum(
        "bhd,bhde->bhe", queries, retention_state, precision=lax.Precision.HIGHEST
    )
    result = own_term + carried
    new_state = (
        decays[None, :, None, None] * retention_state
        + key_rows[:, :, :, None] * values[:, :, None, :]
    )
    normed = result * lax.rsqrt(jnp.mean(result * result, -1, keepdims=True) + GROUP_EPS)
    mixed_heads = (
        normed.reshape(row_count, head_count * head_width) * jax.nn.silu(gate_act)
    ).astype(jnp.bfloat16)
    return (mixed_heads, new_state)


def slot_numbers(route_ids, expert_count, capacity):
    onehot = (route_ids[..., None] == jnp.arange(expert_count, dtype=jnp.int32)).astype(jnp.int32)
    position = jnp.sum(jnp.cumsum(onehot, -2) * onehot, -1) - 1
    return route_ids * capacity + position


def on_device(
    tokens,
    retention_state,
    lengths,
    query_weight,
    key_weight,
    value_weight,
    gate_weight,
    out_weight,
    first_gain,
    routing,
    route_weight,
    expert_gate,
    expert_up,
    expert_down,
    shared_gate,
    shared_up,
    shared_down,
    side_gate,
    side_up,
    side_down,
    side_switch,
    second_gain,
):
    seq_rows = tokens.shape[0]
    model_width = tokens.shape[1]
    head_count = retention_state.shape[1]
    col_count = out_weight.shape[1]
    ep_count = lax.axis_size("ep")
    tp_rank = lax.axis_index("tp")
    col_start = tp_rank * col_count
    mixed_heads, new_state = retain(
        tokens,
        retention_state,
        lengths,
        query_weight,
        key_weight,
        value_weight,
        gate_weight,
        tp_rank * head_count,
    )
    mixing = jnp.dot(
        lax.all_gather(mixed_heads, "tp", axis=1, tiled=True),
        out_weight,
        preferred_element_type=jnp.float32,
    )
    own_cols = lax.dynamic_slice_in_dim(tokens, col_start, col_count, 1).astype(jnp.float32)
    pre_first = RESIDUAL_SCALE * own_cols + mixing
    whole_rows = lax.all_gather(pre_first, "tp", axis=1, tiled=True)
    row_mean = jnp.mean(whole_rows, -1, keepdims=True)
    square = jnp.mean(whole_rows * whole_rows, -1, keepdims=True)
    normed_full = (
        (whole_rows - row_mean) * lax.rsqrt(square - row_mean * row_mean + NORM_EPS) * first_gain
    ).astype(jnp.bfloat16)
    normed_cols = lax.dynamic_slice_in_dim(normed_full, col_start, col_count, 1)
    side_pre = jnp.dot(
        normed_full,
        lax.all_gather(side_gate, "ep", axis=0, tiled=True),
        preferred_element_type=jnp.float32,
    )
    side_lift = jnp.dot(
        normed_full,
        lax.all_gather(side_up, "ep", axis=0, tiled=True),
        preferred_element_type=jnp.float32,
    )
    side_hidden = (jax.nn.silu(side_pre) * side_lift).astype(jnp.bfloat16)
    shared_hidden = (
        jax.nn.silu(jnp.dot(normed_full, shared_gate, preferred_element_type=jnp.float32))
        * jnp.dot(normed_full, shared_up, preferred_element_type=jnp.float32)
    ).astype(jnp.bfloat16)
    shared_all, side_all = (
        lax.all_gather(shared_hidden, "tp", axis=1, tiled=True),
        lax.all_gather(side_hidden, "tp", axis=1, tiled=True),
    )
    shared_out = jnp.dot(shared_all, shared_down, preferred_element_type=jnp.float32)
    side_out = jnp.dot(side_all, side_down, preferred_element_type=jnp.float32)
    switch = jax.nn.sigmoid(jnp.dot(normed_full, side_switch, preferred_element_type=jnp.float32))
    top_count = routing.shape[1]
    local_experts = expert_gate.shape[0]
    expert_count = local_experts * ep_count
    capacity = (3 * seq_rows * top_count + expert_count - 1) // expert_count
    assigned = seq_rows * top_count
    slot_ids = slot_numbers(routing.reshape(assigned), expert_count, capacity)
    slot_hot = (
        slot_ids[:, None] == jnp.arange(expert_count * capacity, dtype=jnp.int32)[None, :]
    ).astype(jnp.bfloat16)
    token_hot = (
        (jnp.arange(assigned, dtype=jnp.int32) // top_count)[:, None]
        == jnp.arange(seq_rows, dtype=jnp.int32)[None, :]
    ).astype(jnp.bfloat16)
    every_rows, every_route = (
        lax.all_gather(normed_full, "ep", axis=0, tiled=True),
        lax.all_gather(routing, "ep", axis=0, tiled=True),
    )
    groups = every_route.reshape(ep_count, assigned)
    local_slot = (
        slot_numbers(groups, expert_count, capacity)
        - lax.axis_index("ep") * local_experts * capacity
    )
    local_hot = (
        local_slot[:, :, None]
        == jnp.arange(local_experts * capacity, dtype=jnp.int32)[None, None, :]
    ).astype(jnp.bfloat16)
    local_table = jnp.einsum(
        "gal,at->glt", local_hot, token_hot, preferred_element_type=jnp.float32
    ).astype(jnp.bfloat16)
    chosen = jnp.einsum(
        "glt,gtd->gld",
        local_table,
        every_rows.reshape(ep_count, seq_rows, model_width),
        preferred_element_type=jnp.float32,
    ).astype(jnp.bfloat16)
    slot_rows = chosen.reshape(ep_count * local_experts, capacity, model_width)
    slot_count = slot_rows.shape[1]
    grouped = slot_rows.reshape(ep_count, local_experts, slot_count, slot_rows.shape[2])
    gate_part = jnp.einsum(
        "sjcd,jdf->sjcf", grouped, expert_gate, preferred_element_type=jnp.float32
    )
    up_part = jnp.einsum("sjcd,jdf->sjcf", grouped, expert_up, preferred_element_type=jnp.float32)
    hidden = (jax.nn.silu(gate_part) * up_part).astype(jnp.bfloat16)
    hidden_all = lax.all_gather(hidden, "tp", axis=3, tiled=True)
    result = jnp.einsum(
        "sjcf,jfd->sjcd", hidden_all, expert_down, preferred_element_type=jnp.float32
    ).astype(jnp.bfloat16)
    returned = lax.all_to_all(
        result.reshape(ep_count * local_experts, slot_count, col_count),
        "ep",
        split_axis=0,
        concat_axis=0,
        tiled=True,
    )
    picked = jnp.dot(
        slot_hot,
        returned.reshape(expert_count * capacity, col_count),
        preferred_element_type=jnp.float32,
    ).reshape(seq_rows, top_count, col_count)
    routed = jnp.sum(picked * route_weight[:, :, None], 1)
    pre_second = (
        RESIDUAL_SCALE * normed_cols.astype(jnp.float32)
        + routed
        + shared_out
        + switch[:, None] * side_out
    )
    totals_second = lax.psum((jnp.sum(pre_second, -1), jnp.sum(pre_second * pre_second, -1)), "tp")
    mean_second = totals_second[0][:, None] / model_width
    square_second = totals_second[1][:, None] / model_width
    output = (
        (pre_second - mean_second)
        * lax.rsqrt(square_second - mean_second * mean_second + NORM_EPS)
        * second_gain
    ).astype(jnp.bfloat16)
    return (output, new_state)


def solution(mesh):
    return jax.shard_map(
        on_device,
        mesh=mesh,
        in_specs=(
            P("ep", None),
            P("ep", "tp", None, None),
            P("ep"),
            P(None, "tp"),
            P(None, "tp"),
            P(None, "tp"),
            P(None, "tp"),
            P(None, "tp"),
            P(),
            P("ep", None),
            P("ep", None),
            P("ep", None, "tp"),
            P("ep", None, "tp"),
            P("ep", None, "tp"),
            P(None, "tp"),
            P(None, "tp"),
            P(None, "tp"),
            P("ep", "tp"),
            P("ep", "tp"),
            P(None, "tp"),
            P(),
            P("tp"),
        ),
        out_specs=(P("ep", "tp"), P("ep", "tp", None, None)),
        check_vma=False,
    )
```

profile of v0, /device:TPU:0, one launch (start us, length us, event | category | flops | bytes accessed | tf_op | source)
XLA Modules:
  0.0 177.6 jit_solution(16361127171532134262)
XLA Ops:
  7.3 0.8 convert_element_type.78
  8.1 2.3 %convolution_convert_fusion.5 = bf16[48,256]{1,0:T(8,128)(2,1)} fusion(bf16[48,2048]{1,0:T(8,128)(2,1)} %param.22, bf16[2048,256]{1,0:T(8,128)(2,1)} %param.25), kind=kOutput, calls=%fused_computation.27 | convolution fusion | flops 50343936 | bytes 1269760 | tf_op jit(solution)/shard_map/dot_general | solution.py:45
  10.4 2.2 %convolution_convert_fusion.4 = bf16[48,256]{1,0:T(8,128)(2,1)} fusion(bf16[48,2048]{1,0:T(8,128)(2,1)} %param.22, bf16[2048,256]{1,0:T(8,128)(2,1)} %param.26), kind=kOutput, calls=%fused_computation.26 | convolution fusion | flops 50343936 | bytes 1269760 | tf_op jit(solution)/shard_map/dot_general | solution.py:45
  13.0 0.9 convolution_convert_fusion.2
  14.0 0.8 reshape.271
  14.9 0.8 reshape.269
  16.3 7.5 %fusion.59 = f32[48,4,1,64]{3,2,1,0:T(1,128)S(1)} fusion(f32[48,4,64,1]{2,3,1,0:T(1,128)S(1)} %bitcast.130, f32[48,4,64,64]{3,2,1,0:T(8,128)} %param.23), kind=kOutput, calls=%fused_computation.105 | convolution fusion | flops 9437184 | bytes 3244032 | tf_op jit(solution)/shard_map/bhd,bhde->bhe/dot_general | solution.py:57
  24.1 0.8 broadcast_multiply_fusion
  24.9 1.6 reshape.259
  26.5 0.8 fusion.47
  27.3 10.9 %all_gather.27 = bf16[48,1024]{1,0:T(8,128)(2,1)} all-gather(bf16[48,256]{1,0:T(8,128)(2,1)S(1)} %fusion.47), channel_id=1, replica_groups=mesh['ep'=8,'tp'=4] {'tp'}, dimensions={1}, use_global_device_ids=true | all-gather | bytes 122880 | tf_op jit(solution)/shard_map/all_gather | solution.py:120
  38.2 1.2 convolution_add_fusion
  39.4 9.4 %all_gather.28 = f32[48,2048]{1,0:T(8,128)S(1)} all-gather(f32[48,512]{1,0:T(8,128)S(1)} %convolution_add_fusion), channel_id=1, replica_groups=mesh['ep'=8,'tp'=4] {'tp'}, dimensions={1}, use_global_device_ids=true | all-gather | bytes 491520 | tf_op jit(solution)/shard_map/all_gather | solution.py:126
  49.0 0.8 multiply_convert_fusion
  49.9 13.2 %all-gather = s32[8,48,4]{1,2,0:T(4,128)S(1)} all-gather(s32[1,48,4]{1,2,0:T(4,128)S(1)} %bitcast.133), channel_id=1, replica_groups=mesh['ep'=8,'tp'=4] {'ep'}, dimensions={0}, use_global_device_ids=true | all-gather | bytes 6912 | tf_op jit(solution)/shard_map/all_gather | solution.py:170
  63.3 0.6 copy-done.14
  63.8 0.6 reduce-window.14
  65.0 0.6 slice.35
  65.9 4.6 %reduce-window.16 = s32[8,32,2,128]{3,1,2,0:T(8,128)S(1)} reduce-window(s32[8,32,2,128]{3,1,2,0:T(8,128)S(1)} %copy_bitcast_fusion, s32[]{:T(128)} %constant.71.clone.1), window={size=1x1x1x128 pad=0_0x0_0x0_0x127_0}, to_apply=%region_7.8 | reduce-window | flops 8323072 | bytes 524292 | tf_op jit(solution)/shard_map/reduce-window.2
  70.9 0.6 and_select_fusion
  71.5 0.8 bitcast_bitcast_fusion.1
  72.3 0.7 fusion.52
  73.0 14.4 %all_gather.33 = bf16[2048,64]{0,1:T(8,128)(2,1)S(1)} all-gather(bf16[256,64]{0,1:T(8,128)(2,1)} %param.39), channel_id=1, replica_groups=mesh['ep'=8,'tp'=4] {'ep'}, dimensions={0}, use_global_device_ids=true | all-gather | bytes 294912 | tf_op jit(solution)/shard_map/all_gather | solution.py:135
  87.4 14.6 %all_gather.34 = bf16[2048,64]{0,1:T(8,128)(2,1)S(1)} all-gather(bf16[256,64]{0,1:T(8,128)(2,1)} %param.40), channel_id=1, replica_groups=mesh['ep'=8,'tp'=4] {'ep'}, dimensions={0}, use_global_device_ids=true | all-gather | bytes 294912 | tf_op jit(solution)/shard_map/all_gather | solution.py:140
  102.2 0.6 broadcast_add_fusion
  102.7 0.8 fusion.61
  104.0 3.8 %convolution_convert_fusion = bf16[8,72,2048]{2,1,0:T(8,128)(2,1)} fusion(bf16[8,48,2048]{2,1,0:T(8,128)(2,1)} %bitcast.129, s32[8,192]{1,0:T(8,128)S(1)} %add_subtract_fusion, s32[192]{0:T(256)} %and_select_fusion), kind=kOutput, calls=%fused_computation.2 | convolution fusion | flops 125190144 | bytes 3939072 | tf_op jit(solution)/shard_map/glt,gtd->gld/dot_general | solution.py:184
  107.9 3.1 %copy.95 = bf16[8,72,2048]{2,0,1:T(8,128)(2,1)S(1)} copy(bf16[8,72,2048]{2,1,0:T(8,128)(2,1)} %convolution_convert_fusion) | data formatting | bytes 4718592 | tf_op jit(solution)/shard_map/convert_element_type | solution.py:189
  111.0 0.8 fusion.13
  111.8 0.8 copy-done.18
  112.6 0.8 fusion.23
  113.4 10.4 %all_gather.31 = bf16[8,4,18,512]{3,0,2,1:T(8,128)(2,1)S(1)} all-gather(bf16[8,4,18,128]{3,0,2,1:T(8,128)(2,1)S(1)} %fusion.23), channel_id=1, replica_groups=mesh['ep'=8,'tp'=4] {'tp'}, dimensions={3}, use_global_device_ids=true | all-gather | bytes 737280 | tf_op jit(solution)/shard_map/all_gather | solution.py:198
  123.8 0.7 fusion.10
  124.5 0.9 copy.105
  125.5 3.5 %all-to-all-start = ((bf16[32,18,512]{2,1,0:T(8,128)(2,1)}), bf16[32,18,512]{2,1,0:T(8,128)(2,1)S(1)}, u32[]{:S(2)}, u32[]{:S(2)}) async-start(bf16[32,18,512]{2,1,0:T(8,128)(2,1)} %bitcast.22), calls=%async_computation | async-start | bytes 1572864 | tf_op jit(solution)/shard_map/all_to_all | solution.py:202
  129.0 1.6 fusion.31
  130.6 0.7 reshape.288
  131.3 0.8 sub.90
  132.1 7.6 %all-gather.1 = bf16[4,64,48]{1,2,0:T(8,128)(2,1)S(1)} all-gather(bf16[1,64,48]{1,2,0:T(8,128)(2,1)} %fusion.31), channel_id=1, replica_groups=mesh['ep'=8,'tp'=4] {'tp'}, dimensions={0}, use_global_device_ids=true | all-gather | bytes 30720 | tf_op jit(solution)/shard_map/all_gather | solution.py:150
  139.8 0.7 reshape.279
  140.5 8.4 %all_gather.32 = bf16[48,512]{1,0:T(8,128)(2,1)} all-gather(bf16[48,128]{1,0:T(8,128)(2,1)S(1)} %fusion.29), channel_id=1, replica_groups=mesh['ep'=8,'tp'=4] {'tp'}, dimensions={1}, use_global_device_ids=true | all-gather | bytes 61440 | tf_op jit(solution)/shard_map/all_gather | solution.py:149
  149.0 7.4 %multiply_add_fusion = f32[48,4,64,64]{3,2,1,0:T(8,128)} fusion(f32[48,4,64,64]{3,2,1,0:T(8,128)} %param.23, f32[48,4,64]{2,1,0:T(4,128)S(1)} %reshape.273, f32[48,4,64]{2,1,0:T(4,128)S(1)} %get-tuple-element.24, f32[4]{0:T(128)} %copy-done.17), kind=kLoop, calls=%fused_computation.1 | loop fusion | flops 2359296 | bytes 6389776 | tf_op jit(solution)/shard_map/add | solution.py:62
  156.4 1.0 reshape.287
  157.4 1.4 fusion.22
  158.9 1.2 convolution_add_fusion.1
  160.1 1.0 fusion.58
  161.1 8.9 %all-reduce.2 = (f32[48]{0:T(128)S(1)}, f32[48]{0:T(128)S(1)}) all-reduce(f32[48]{0:T(128)S(1)} %get-tuple-element.5, f32[48]{0:T(128)S(1)} %get-tuple-element.4), channel_id=1, replica_groups=mesh['ep'=8,'tp'=4] {'tp'}, use_global_device_ids=true, to_apply=%region_14.15 | all-reduce | flops 96 | bytes 768 | tf_op jit(solution)/shard_map/psum | solution.py:221
  170.1 0.7 multiply_convert_fusion.1
  (78 shorter events, 3.9 us)
Async XLA Ops:
  7.2 116.6 %copy-start = (bf16[4,512,512]{2,1,0:T(8,128)(2,1)S(1)}, bf16[4,512,512]{2,1,0:T(8,128)(2,1)}, u32[]{:S(2)}) copy-start(bf16[4,512,512]{2,1,0:T(8,128)(2,1)} %param.35) | copy-start | bytes 6291460
  7.2 5.5 %copy-start.3 = (bf16[48,2048]{1,0:T(8,128)(2,1)S(1)}, bf16[48,2048]{1,0:T(8,128)(2,1)}, u32[]{:S(2)}) copy-start(bf16[48,2048]{1,0:T(8,128)(2,1)} %param.22) | copy-start | bytes 589828
  7.2 5.5 %copy-start.4 = (bf16[2048,256]{1,0:T(8,128)(2,1)S(1)}, bf16[2048,256]{1,0:T(8,128)(2,1)}, u32[]{:S(2)}) copy-start(bf16[2048,256]{1,0:T(8,128)(2,1)} %param.27) | copy-start | bytes 3145732
  7.2 96.8 %all-gather.4.cloned.1.call-start = ((), (), s32[]{:S(2)}) async-start(), calls=%async_computation.1 | async-start | bytes 1769472 | tf_op jit(solution)/shard_map/all_gather | solution.py:169
  7.3 5.7 %copy-start.5 = (bf16[2048,256]{1,0:T(8,128)(2,1)S(1)}, bf16[2048,256]{1,0:T(8,128)(2,1)}, u32[]{:S(2)}) copy-start(bf16[2048,256]{1,0:T(8,128)(2,1)} %param.28) | copy-start | bytes 3145732
  7.3 16.5 %copy-start.17 = (f32[4]{0:T(128)}, f32[4]{0:T(128)S(1)}, u32[]{:S(2)}) copy-start(f32[4]{0:T(128)S(1)} %power_subtract_fusion) | copy-start | bytes 52
  16.3 21.9 %copy-start.6 = (bf16[1024,512]{1,0:T(8,128)(2,1)S(1)}, bf16[1024,512]{1,0:T(8,128)(2,1)}, u32[]{:S(2)}) copy-start(bf16[1024,512]{1,0:T(8,128)(2,1)} %param.29) | copy-start | bytes 3145732
  23.8 25.2 %copy-start.15 = (f32[2048]{0:T(1024)S(1)}, f32[2048]{0:T(1024)}, u32[]{:S(2)}) copy-start(f32[2048]{0:T(1024)} %param.30) | copy-start | bytes 24580
  23.8 26.0 %copy-start.12 = (s32[48,4]{0,1:T(4,128)S(1)}, s32[48,4]{0,1:T(4,128)}, u32[]{:S(2)}) copy-start(s32[48,4]{0,1:T(4,128)} %param.31) | copy-start | bytes 2308
  49.8 53.0 %copy-start.1 = (bf16[48,2048]{1,0:T(8,128)(2,1)S(1)}, bf16[48,2048]{1,0:T(8,128)(2,1)}, u32[]{:S(2)}) copy-start(bf16[48,2048]{1,0:T(8,128)(2,1)} %multiply_convert_fusion) | copy-start | bytes 589828
  49.8 53.8 %copy-start.7 = (bf16[2048,128]{1,0:T(8,128)(2,1)S(1)}, bf16[2048,128]{1,0:T(8,128)(2,1)}, u32[]{:S(2)}) copy-start(bf16[2048,128]{1,0:T(8,128)(2,1)} %param.36) | copy-start | bytes 1572868
  63.3 0.6 copy-start.14
  64.4 0.6 copy-start.9
  70.9 32.9 %copy-start.8 = (bf16[2048,128]{1,0:T(8,128)(2,1)S(1)}, bf16[2048,128]{1,0:T(8,128)(2,1)}, u32[]{:S(2)}) copy-start(bf16[2048,128]{1,0:T(8,128)(2,1)} %param.37) | copy-start | bytes 1572868
  107.9 3.1 %copy-start.2 = (bf16[4,2048,128]{2,1,0:T(8,128)(2,1)S(1)}, bf16[4,2048,128]{2,1,0:T(8,128)(2,1)}, u32[]{:S(2)}) copy-start(bf16[4,2048,128]{2,1,0:T(8,128)(2,1)} %param.33) | copy-start | bytes 6291460
  111.0 1.6 copy-start.18
  124.5 24.3 %copy-start.13 = (s32[48,4]{0,1:T(4,128)S(1)}, s32[48,4]{0,1:T(4,128)}, u32[]{:S(2)}) copy-start(s32[48,4]{0,1:T(4,128)} %param.31) | copy-start | bytes 2308
  125.5 30.9 %all-to-all-start = ((bf16[32,18,512]{2,1,0:T(8,128)(2,1)}), bf16[32,18,512]{2,1,0:T(8,128)(2,1)S(1)}, u32[]{:S(2)}, u32[]{:S(2)}) async-start(bf16[32,18,512]{2,1,0:T(8,128)(2,1)} %bitcast.22), calls=%async_computation | async-start | bytes 1572864 | tf_op jit(solution)/shard_map/all_to_all | solution.py:202
  149.0 8.4 %copy-start.19 = (f32[48,4]{0,1:T(4,128)S(1)}, f32[48,4]{0,1:T(4,128)}, u32[]{:S(2)}) copy-start(f32[48,4]{0,1:T(4,128)} %param.32) | copy-start | bytes 2308
  156.4 2.5 %copy-start.11 = (bf16[48,512]{1,0:T(8,128)(2,1)S(1)}, bf16[48,512]{1,0:T(8,128)(2,1)}, u32[]{:S(2)}) copy-start(bf16[48,512]{1,0:T(8,128)(2,1)} %all_gather.32) | copy-start | bytes 147460
  156.4 3.7 %copy-start.10 = (bf16[256,512]{1,0:T(8,128)(2,1)S(1)}, bf16[256,512]{1,0:T(8,128)(2,1)}, u32[]{:S(2)}) copy-start(bf16[256,512]{1,0:T(8,128)(2,1)} %param.41) | copy-start | bytes 786436
  156.4 13.7 %copy-start.16 = (f32[512]{0:T(512)S(1)}, f32[512]{0:T(512)}, u32[]{:S(2)}) copy-start(f32[512]{0:T(512)} %param.43) | copy-start | bytes 6148
Sparse Core Ops, SparseCore 0:
  49.9 25.5 all-gather.3
where the time goes:
time: 179 us; the launch traced here: 178 us
  blocking collectives  97.9 us (55%)
  matrix products  27.1 us (15%)
  other arithmetic  20.6 us (12%)
  between operations  14.5 us (8%)
  local copies, waits for them, and re-layouts  14 us (8%)
  starting transfers between devices  3.58 us (2%)
    all_gather x1, blocking collectives, on_device(): lax.all_gather(side_up, 'ep', axis=0, tiled=True)  14.6 us
    all_gather x1, blocking collectives, on_device(): lax.all_gather(side_gate, 'ep', axis=0, tiled=True)  14.4 us
    all_gather x1, blocking collectives, on_device(): lax.all_gather(routing, 'ep', axis=0, tiled=True)  13.2 us
    all_gather x1, blocking collectives, on_device(): lax.all_gather(mixed_heads, 'tp', axis=1, tiled=True)  10.9 us
    all_gather x1, blocking collectives, on_device(): hidden_all = lax.all_gather(hidden, 'tp', axis=3, tiled=True)  10.4 us
    all_gather x1, blocking collectives, on_device(): whole_rows = lax.all_gather(pre_first, 'tp', axis=1, tiled=True)  9.44 us
    psum x1, blocking collectives, on_device(): lax.psum((jnp.sum(pre_second, -1), jnp.sum(pre_second * pre_second, -1)),...  8.93 us
    all_gather x1, blocking collectives, on_device(): lax.all_gather(shared_hidden, 'tp', axis=1, tiled=True)  8.35 us
  transfers between devices with their start and end apart: 2, of which 0 were waited for; matrix products, arithmetic and copies ran while one was open for 13% of the time, Pallas kernels for 0%

commit v1 on v0

--- a/solution.py
+++ b/solution.py
@@ -117,7 +117,7 @@
         tp_rank * head_count,
     )
     mixing = jnp.dot(
-        lax.all_gather(mixed_heads, "tp", axis=1, tiled=True),
+        jnp.concatenate(lax.all_gather(mixed_heads, "tp"), axis=1),
         out_weight,
         preferred_element_type=jnp.float32,
     )

time: 179 us -> 178 us (level)
    unnamed x43 -> x44, local copies, waits for them, and re-layouts: 3.35 us -> 4.01 us
where the time goes in v1:
time: 178 us; the launch traced here: 177 us
  blocking collectives  96.8 us (54%)
  matrix products  27.1 us (15%)
  other arithmetic  20.6 us (12%)
  local copies, waits for them, and re-layouts  14.7 us (8%)
  between operations  14.5 us (8%)
  starting transfers between devices  3.58 us (2%)
    all_gather x1, blocking collectives, on_device(): lax.all_gather(side_up, 'ep', axis=0, tiled=True)  14.6 us
    all_gather x1, blocking collectives, on_device(): lax.all_gather(side_gate, 'ep', axis=0, tiled=True)  14.4 us
    all_gather x1, blocking collectives, on_device(): lax.all_gather(routing, 'ep', axis=0, tiled=True)  13.2 us
    all_gather x1, blocking collectives, on_device(): hidden_all = lax.all_gather(hidden, 'tp', axis=3, tiled=True)  10.4 us
    all_gather x1, blocking collectives, on_device(): lax.all_gather(mixed_heads, 'tp')  9.84 us
    all_gather x1, blocking collectives, on_device(): whole_rows = lax.all_gather(pre_first, 'tp', axis=1, tiled=True)  9.49 us
    psum x1, blocking collectives, on_device(): lax.psum((jnp.sum(pre_second, -1), jnp.sum(pre_second * pre_second, -1)),...  8.93 us
    all_gather x1, blocking collectives, on_device(): lax.all_gather(shared_hidden, 'tp', axis=1, tiled=True)  8.3 us
  transfers between devices with their start and end apart: 2, of which 0 were waited for; matrix products, arithmetic and copies ran while one was open for 13% of the time, Pallas kernels for 0%

profile of v1, /device:TPU:0, one launch (start us, length us, event | category | flops | bytes accessed | tf_op | source)
XLA Modules:
  0.0 177.3 jit_solution(6277647999311556806)
XLA Ops:
  7.3 0.8 convert_element_type.78
  8.1 2.3 %convolution_convert_fusion.5 = bf16[48,256]{1,0:T(8,128)(2,1)} fusion(bf16[48,2048]{1,0:T(8,128)(2,1)} %param.22, bf16[2048,256]{1,0:T(8,128)(2,1)} %param.25), kind=kOutput, calls=%fused_computation.27 | convolution fusion | flops 50343936 | bytes 1269760 | tf_op jit(solution)/shard_map/dot_general | solution.py:45
  10.4 2.2 %convolution_convert_fusion.4 = bf16[48,256]{1,0:T(8,128)(2,1)} fusion(bf16[48,2048]{1,0:T(8,128)(2,1)} %param.22, bf16[2048,256]{1,0:T(8,128)(2,1)} %param.26), kind=kOutput, calls=%fused_computation.26 | convolution fusion | flops 50343936 | bytes 1269760 | tf_op jit(solution)/shard_map/dot_general | solution.py:45
  13.0 0.9 convolution_convert_fusion.2
  14.0 0.8 reshape.279
  14.9 0.8 reshape.277
  16.3 7.5 %fusion.59 = f32[48,4,1,64]{3,2,1,0:T(1,128)S(1)} fusion(f32[48,4,64,1]{2,3,1,0:T(1,128)S(1)} %bitcast.134, f32[48,4,64,64]{3,2,1,0:T(8,128)} %param.23), kind=kOutput, calls=%fused_computation.105 | convolution fusion | flops 9437184 | bytes 3244032 | tf_op jit(solution)/shard_map/bhd,bhde->bhe/dot_general | solution.py:57
  24.1 0.8 broadcast_multiply_fusion
  24.9 1.6 reshape.265
  26.5 0.8 fusion.47
  27.3 9.8 %all-gather = bf16[192,256]{1,0:T(8,128)(2,1)S(1)} all-gather(bf16[48,256]{1,0:T(8,128)(2,1)S(1)} %fusion.47), channel_id=2, replica_groups=mesh['ep'=8,'tp'=4] {'tp'}, dimensions={0}, use_global_device_ids=true | all-gather | bytes 122880 | tf_op jit(solution)/shard_map/all_gather | solution.py:120
  37.2 0.7 copy.115
  37.9 1.2 convolution_add_fusion
  39.1 9.5 %all_gather.32 = f32[48,2048]{1,0:T(8,128)S(1)} all-gather(f32[48,512]{1,0:T(8,128)S(1)} %convolution_add_fusion), channel_id=1, replica_groups=mesh['ep'=8,'tp'=4] {'tp'}, dimensions={1}, use_global_device_ids=true | all-gather | bytes 491520 | tf_op jit(solution)/shard_map/all_gather | solution.py:126
  48.7 0.8 multiply_convert_fusion
  49.6 13.2 %all-gather.1 = s32[8,48,4]{1,2,0:T(4,128)S(1)} all-gather(s32[1,48,4]{1,2,0:T(4,128)S(1)} %bitcast.140), channel_id=1, replica_groups=mesh['ep'=8,'tp'=4] {'ep'}, dimensions={0}, use_global_device_ids=true | all-gather | bytes 6912 | tf_op jit(solution)/shard_map/all_gather | solution.py:170
  63.6 0.6 reduce-window.14
  64.8 0.6 slice.35
  65.6 4.6 %reduce-window.16 = s32[8,32,2,128]{3,1,2,0:T(8,128)S(1)} reduce-window(s32[8,32,2,128]{3,1,2,0:T(8,128)S(1)} %copy_bitcast_fusion, s32[]{:T(128)} %constant.71.clone.1), window={size=1x1x1x128 pad=0_0x0_0x0_0x127_0}, to_apply=%region_7.8 | reduce-window | flops 8323072 | bytes 524292 | tf_op jit(solution)/shard_map/reduce-window.2
  70.6 0.6 and_select_fusion
  71.2 0.8 bitcast_bitcast_fusion.1
  72.0 0.7 fusion.52
  72.7 14.4 %all_gather.37 = bf16[2048,64]{0,1:T(8,128)(2,1)S(1)} all-gather(bf16[256,64]{0,1:T(8,128)(2,1)} %param.39), channel_id=1, replica_groups=mesh['ep'=8,'tp'=4] {'ep'}, dimensions={0}, use_global_device_ids=true | all-gather | bytes 294912 | tf_op jit(solution)/shard_map/all_gather | solution.py:135
  87.1 14.6 %all_gather.38 = bf16[2048,64]{0,1:T(8,128)(2,1)S(1)} all-gather(bf16[256,64]{0,1:T(8,128)(2,1)} %param.40), channel_id=1, replica_groups=mesh['ep'=8,'tp'=4] {'ep'}, dimensions={0}, use_global_device_ids=true | all-gather | bytes 294912 | tf_op jit(solution)/shard_map/all_gather | solution.py:140
  101.9 0.6 broadcast_add_fusion
  102.5 0.8 fusion.61
  103.8 3.8 %convolution_convert_fusion = bf16[8,72,2048]{2,1,0:T(8,128)(2,1)} fusion(bf16[8,48,2048]{2,1,0:T(8,128)(2,1)} %bitcast.133, s32[8,192]{1,0:T(8,128)S(1)} %add_subtract_fusion, s32[192]{0:T(256)} %and_select_fusion), kind=kOutput, calls=%fused_computation.2 | convolution fusion | flops 125190144 | bytes 3939072 | tf_op jit(solution)/shard_map/glt,gtd->gld/dot_general | solution.py:184
  107.6 3.1 %copy.99 = bf16[8,72,2048]{2,0,1:T(8,128)(2,1)S(1)} copy(bf16[8,72,2048]{2,1,0:T(8,128)(2,1)} %convolution_convert_fusion) | data formatting | bytes 4718592 | tf_op jit(solution)/shard_map/convert_element_type | solution.py:189
  110.7 0.8 fusion.13
  111.5 0.8 copy-done.18
  112.3 0.8 fusion.23
  113.1 10.4 %all_gather.35 = bf16[8,4,18,512]{3,0,2,1:T(8,128)(2,1)S(1)} all-gather(bf16[8,4,18,128]{3,0,2,1:T(8,128)(2,1)S(1)} %fusion.23), channel_id=1, replica_groups=mesh['ep'=8,'tp'=4] {'tp'}, dimensions={3}, use_global_device_ids=true | all-gather | bytes 737280 | tf_op jit(solution)/shard_map/all_gather | solution.py:198
  123.5 0.7 fusion.10
  124.2 0.9 copy.109
  125.1 3.5 %all-to-all-start = ((bf16[32,18,512]{2,1,0:T(8,128)(2,1)}), bf16[32,18,512]{2,1,0:T(8,128)(2,1)S(1)}, u32[]{:S(2)}, u32[]{:S(2)}) async-start(bf16[32,18,512]{2,1,0:T(8,128)(2,1)} %bitcast.24), calls=%async_computation | async-start | bytes 1572864 | tf_op jit(solution)/shard_map/all_to_all | solution.py:202
  128.7 1.6 fusion.31
  130.2 0.7 reshape.297
  130.9 0.8 sub.90
  131.8 7.7 %all-gather.2 = bf16[4,64,48]{1,2,0:T(8,128)(2,1)S(1)} all-gather(bf16[1,64,48]{1,2,0:T(8,128)(2,1)} %fusion.31), channel_id=1, replica_groups=mesh['ep'=8,'tp'=4] {'tp'}, dimensions={0}, use_global_device_ids=true | all-gather | bytes 30720 | tf_op jit(solution)/shard_map/all_gather | solution.py:150
  139.5 0.7 reshape.288
  140.2 8.3 %all_gather.36 = bf16[48,512]{1,0:T(8,128)(2,1)} all-gather(bf16[48,128]{1,0:T(8,128)(2,1)S(1)} %fusion.29), channel_id=1, replica_groups=mesh['ep'=8,'tp'=4] {'tp'}, dimensions={1}, use_global_device_ids=true | all-gather | bytes 61440 | tf_op jit(solution)/shard_map/all_gather | solution.py:149
  148.7 7.4 %multiply_add_fusion = f32[48,4,64,64]{3,2,1,0:T(8,128)} fusion(f32[48,4,64,64]{3,2,1,0:T(8,128)} %param.23, f32[48,4,64]{2,1,0:T(4,128)S(1)} %reshape.281, f32[48,4,64]{2,1,0:T(4,128)S(1)} %get-tuple-element.24, f32[4]{0:T(128)} %copy-done.17), kind=kLoop, calls=%fused_computation.1 | loop fusion | flops 2359296 | bytes 6389776 | tf_op jit(solution)/shard_map/add | solution.py:62
  156.1 1.0 reshape.296
  157.1 1.4 fusion.22
  158.5 1.2 convolution_add_fusion.1
  159.8 1.0 fusion.58
  160.8 8.9 %all-reduce.2 = (f32[48]{0:T(128)S(1)}, f32[48]{0:T(128)S(1)}) all-reduce(f32[48]{0:T(128)S(1)} %get-tuple-element.5, f32[48]{0:T(128)S(1)} %get-tuple-element.4), channel_id=1, replica_groups=mesh['ep'=8,'tp'=4] {'tp'}, use_global_device_ids=true, to_apply=%region_14.15 | all-reduce | flops 96 | bytes 768 | tf_op jit(solution)/shard_map/psum | solution.py:221
  169.8 0.7 multiply_convert_fusion.1
  (80 shorter events, 4.5 us)
Async XLA Ops:
  7.2 116.3 %copy-start = (bf16[4,512,512]{2,1,0:T(8,128)(2,1)S(1)}, bf16[4,512,512]{2,1,0:T(8,128)(2,1)}, u32[]{:S(2)}) copy-start(bf16[4,512,512]{2,1,0:T(8,128)(2,1)} %param.35) | copy-start | bytes 6291460
  7.2 5.5 %copy-start.3 = (bf16[48,2048]{1,0:T(8,128)(2,1)S(1)}, bf16[48,2048]{1,0:T(8,128)(2,1)}, u32[]{:S(2)}) copy-start(bf16[48,2048]{1,0:T(8,128)(2,1)} %param.22) | copy-start | bytes 589828
  7.2 5.5 %copy-start.4 = (bf16[2048,256]{1,0:T(8,128)(2,1)S(1)}, bf16[2048,256]{1,0:T(8,128)(2,1)}, u32[]{:S(2)}) copy-start(bf16[2048,256]{1,0:T(8,128)(2,1)} %param.27) | copy-start | bytes 3145732
  7.2 96.6 %all-gather.5.cloned.1.call-start = ((), (), s32[]{:S(2)}) async-start(), calls=%async_computation.1 | async-start | bytes 1769472 | tf_op jit(solution)/shard_map/all_gather | solution.py:169
  7.3 5.7 %copy-start.5 = (bf16[2048,256]{1,0:T(8,128)(2,1)S(1)}, bf16[2048,256]{1,0:T(8,128)(2,1)}, u32[]{:S(2)}) copy-start(bf16[2048,256]{1,0:T(8,128)(2,1)} %param.28) | copy-start | bytes 3145732
  7.3 16.5 %copy-start.17 = (f32[4]{0:T(128)}, f32[4]{0:T(128)S(1)}, u32[]{:S(2)}) copy-start(f32[4]{0:T(128)S(1)} %power_subtract_fusion) | copy-start | bytes 52
  16.3 21.5 %copy-start.6 = (bf16[1024,512]{1,0:T(8,128)(2,1)S(1)}, bf16[1024,512]{1,0:T(8,128)(2,1)}, u32[]{:S(2)}) copy-start(bf16[1024,512]{1,0:T(8,128)(2,1)} %param.29) | copy-start | bytes 3145732
  23.8 24.9 %copy-start.15 = (f32[2048]{0:T(1024)S(1)}, f32[2048]{0:T(1024)}, u32[]{:S(2)}) copy-start(f32[2048]{0:T(1024)} %param.30) | copy-start | bytes 24580
  23.8 25.7 %copy-start.12 = (s32[48,4]{0,1:T(4,128)S(1)}, s32[48,4]{0,1:T(4,128)}, u32[]{:S(2)}) copy-start(s32[48,4]{0,1:T(4,128)} %param.31) | copy-start | bytes 2308
  49.5 53.0 %copy-start.1 = (bf16[48,2048]{1,0:T(8,128)(2,1)S(1)}, bf16[48,2048]{1,0:T(8,128)(2,1)}, u32[]{:S(2)}) copy-start(bf16[48,2048]{1,0:T(8,128)(2,1)} %multiply_convert_fusion) | copy-start | bytes 589828
  49.5 53.8 %copy-start.7 = (bf16[2048,128]{1,0:T(8,128)(2,1)S(1)}, bf16[2048,128]{1,0:T(8,128)(2,1)}, u32[]{:S(2)}) copy-start(bf16[2048,128]{1,0:T(8,128)(2,1)} %param.36) | copy-start | bytes 1572868
  63.0 0.6 copy-start.14
  64.1 0.6 copy-start.9
  70.6 32.9 %copy-start.8 = (bf16[2048,128]{1,0:T(8,128)(2,1)S(1)}, bf16[2048,128]{1,0:T(8,128)(2,1)}, u32[]{:S(2)}) copy-start(bf16[2048,128]{1,0:T(8,128)(2,1)} %param.37) | copy-start | bytes 1572868
  107.6 3.1 %copy-start.2 = (bf16[4,2048,128]{2,1,0:T(8,128)(2,1)S(1)}, bf16[4,2048,128]{2,1,0:T(8,128)(2,1)}, u32[]{:S(2)}) copy-start(bf16[4,2048,128]{2,1,0:T(8,128)(2,1)} %param.33) | copy-start | bytes 6291460
  110.7 1.6 copy-start.18
  124.2 24.3 %copy-start.13 = (s32[48,4]{0,1:T(4,128)S(1)}, s32[48,4]{0,1:T(4,128)}, u32[]{:S(2)}) copy-start(s32[48,4]{0,1:T(4,128)} %param.31) | copy-start | bytes 2308
  125.1 30.9 %all-to-all-start = ((bf16[32,18,512]{2,1,0:T(8,128)(2,1)}), bf16[32,18,512]{2,1,0:T(8,128)(2,1)S(1)}, u32[]{:S(2)}, u32[]{:S(2)}) async-start(bf16[32,18,512]{2,1,0:T(8,128)(2,1)} %bitcast.24), calls=%async_computation | async-start | bytes 1572864 | tf_op jit(solution)/shard_map/all_to_all | solution.py:202
  148.7 8.4 %copy-start.19 = (f32[48,4]{0,1:T(4,128)S(1)}, f32[48,4]{0,1:T(4,128)}, u32[]{:S(2)}) copy-start(f32[48,4]{0,1:T(4,128)} %param.32) | copy-start | bytes 2308
  156.1 2.5 %copy-start.11 = (bf16[48,512]{1,0:T(8,128)(2,1)S(1)}, bf16[48,512]{1,0:T(8,128)(2,1)}, u32[]{:S(2)}) copy-start(bf16[48,512]{1,0:T(8,128)(2,1)} %all_gather.36) | copy-start | bytes 147460
  156.1 3.7 %copy-start.10 = (bf16[256,512]{1,0:T(8,128)(2,1)S(1)}, bf16[256,512]{1,0:T(8,128)(2,1)}, u32[]{:S(2)}) copy-start(bf16[256,512]{1,0:T(8,128)(2,1)} %param.41) | copy-start | bytes 786436
  156.1 13.7 %copy-start.16 = (f32[512]{0:T(512)S(1)}, f32[512]{0:T(512)}, u32[]{:S(2)}) copy-start(f32[512]{0:T(512)} %param.43) | copy-start | bytes 6148
Sparse Core Ops, SparseCore 0:
  49.7 25.5 all-gather.4
